TPU v7x, 512 devices: a whole 4x8x8 slice. The times are simulated.
512 devices in a mesh: sp: 32 (over z, x), dp: 16 (over y, core).
Axes of the slice: x: 4, y: 8, z: 8, core: 2. Of those that a mesh axis runs over, the one named last changes fastest.
Arguments:
- queries: bfloat16 [64, 8, 2048, 256], P('dp', None, 'sp'), may hold values from -6 to 6
- keys: bfloat16 [64, 8, 2048, 256], P('dp', None, 'sp'), may hold values from -6 to 6
- values: bfloat16 [64, 8, 2048, 256], P('dp', None, 'sp'), may hold values from -6 to 6
- log_decay: float32 [512, 2048], P(('dp', 'sp')), may hold values from -2 to 0, as said below
- w_out: bfloat16 [8, 256, 2048], P(None, None, 'dp'), may hold values from -0.125 to 0.125
Outputs:
- mixed_out: bfloat16 [64, 2048, 2048], P('dp', 'sp')
Inputs may be any that keep to these rules, and one draw needn't show every extreme that they name: Every entry of log_decay is below zero.
All inputs are finite; a program needn't handle non-finite values.
Results may differ from a plain program's by a relative error of at most 0.008.
Values may be sent and summed in bfloat16 or wider, within the bound.
A program may use at most 128 MiB of HBM per device.

v0:
```python
import jax
import jax.numpy as jnp
from jax import lax
from jax.sharding import PartitionSpec as P

BLOCK = 64


def in_one_piece(arrays, axis, split_dim, concat_dim, along):
    both = jnp.concatenate(arrays, axis=along)
    whole, at, gathered = (
        lax.all_to_all(both, axis, split_axis=split_dim, concat_axis=concat_dim, tiled=True),
        0,
        [],
    )
    for a in arrays:
        gathered.append(lax.slice_in_dim(whole, at, at + a.shape[along], axis=along))
        at += a.shape[along]
    return tuple(gathered)


def cut_along(value, dim, devices):
    before, after = (value.shape[:dim], value.shape[dim + 1 :])
    return jnp.moveaxis(value.reshape(*before, devices, -1, *after), dim, 0)


def cut_rows(length, count):
    step = length // count
    if step >= 8:
        step -= step % 8
    return [step * k for k in range(1, count)]


def joined_along(parts, dim):
    parts = jnp.moveaxis(parts, 0, dim)
    shape = parts.shape
    return parts.reshape(*shape[:dim], shape[dim] * shape[dim + 1], *shape[dim + 2 :])


def several_exchanges(value, axis, pieces, split_dim, concat_dim):
    parts = cut_along(value, split_dim, lax.axis_size(axis))
    cut = max(range(1, max(2, parts.ndim - 1)), key=lambda d: parts.shape[d])
    gathered = []
    for slab in jnp.split(parts, cut_rows(parts.shape[cut], pieces), axis=cut):
        if slab.size:
            gathered.append(lax.all_to_all(slab, axis, split_axis=0, concat_axis=0, tiled=True))
    return joined_along(jnp.concatenate(gathered, axis=cut), concat_dim)


def rotate(field_in, cosine, sine_tab):
    half_dim = field_in.shape[1] // 2
    widened = field_in.astype(jnp.float32)
    first_half = widened[:, :half_dim]
    second_half = widened[:, half_dim:]
    turned = jnp.concatenate(
        [
            first_half * cosine - second_half * sine_tab,
            second_half * cosine + first_half * sine_tab,
        ],
        axis=1,
    )
    return turned.astype(jnp.bfloat16)


def retain(query_rows, key_rows, value_rows, decay_row, cosine, sine_tab):
    length, head_width = query_rows.shape
    blocks = length // BLOCK
    rot_query = rotate(query_rows, cosine, sine_tab).reshape(blocks, BLOCK, head_width)
    rot_key = rotate(key_rows, cosine, sine_tab).reshape(blocks, BLOCK, head_width)
    value_blocks = value_rows.reshape(blocks, BLOCK, head_width)
    within = jnp.cumsum(decay_row.reshape(blocks, BLOCK), axis=1)
    ending = within[:, -1:]
    causal = jnp.tril(jnp.ones((BLOCK, BLOCK), dtype=bool))[None]
    spread = within[:, :, None] - within[:, None, :]
    decay_mask = jnp.where(causal, jnp.exp(jnp.where(causal, spread, 0.0)), 0.0)
    scores = jnp.einsum("bnd,bmd->bnm", rot_query, rot_key, preferred_element_type=jnp.float32)
    weights = (scores * decay_mask).astype(jnp.bfloat16)
    scaled_keys = (rot_key * jnp.exp(ending - within)[:, :, None]).astype(jnp.bfloat16)
    updates = jnp.einsum(
        "bmd,bme->bde", scaled_keys, value_blocks, preferred_element_type=jnp.float32
    )

    def advance(state_now, inputs):
        factor, update = inputs
        return (factor * state_now + update, state_now.astype(jnp.bfloat16))

    start_state = jnp.zeros((head_width, head_width), jnp.float32)
    _, before = lax.scan(advance, start_state, (jnp.exp(ending[:, 0]), updates))
    local_part = jnp.einsum(
        "bnm,bme->bne", weights, value_blocks, preferred_element_type=jnp.float32
    )
    carried = jnp.einsum("bnd,bde->bne", rot_query, before, preferred_element_type=jnp.float32)
    combined = local_part + jnp.exp(within)[:, :, None] * carried
    return combined.reshape(length, head_width).astype(jnp.bfloat16)


def on_device(queries, keys, values, log_decay, w_out):
    groups, head_count, seg_len, head_width = queries.shape
    item_count = groups * head_count
    whole_w = lax.all_gather(w_out, "dp", axis=2, tiled=True)
    flat_q = queries.reshape(item_count, seg_len, head_width)
    flat_k = keys.reshape(item_count, seg_len, head_width)
    flat_v = values.reshape(item_count, seg_len, head_width)
    head_q, head_k, head_v = in_one_piece((flat_q, flat_k, flat_v), "sp", 0, 1, 2)
    length = head_q.shape[1]
    half_dim = head_width // 2
    frequency = 10000.0 ** (-jnp.arange(half_dim, dtype=jnp.float32) / half_dim)
    angles = jnp.arange(length, dtype=jnp.float32)[:, None] * frequency[None, :]
    cosine = jnp.cos(angles)
    sine_tab = jnp.sin(angles)

    def one_item(inputs):
        return retain(inputs[0], inputs[1], inputs[2], inputs[3], cosine, sine_tab)

    retained = lax.map(one_item, (head_q, head_k, head_v, log_decay))
    by_token = several_exchanges(retained, "sp", 2, 1, 0)
    by_token = by_token.reshape(groups, head_count, seg_len, head_width)
    widened = by_token.astype(jnp.float32)
    normed = (
        widened * lax.rsqrt(jnp.mean(widened * widened, axis=-1, keepdims=True) + 1e-06)
    ).astype(jnp.bfloat16)
    mixed_out = jnp.einsum("shtd,hde->ste", normed, whole_w, preferred_element_type=jnp.float32)
    return mixed_out.astype(jnp.bfloat16)


def solution(mesh):
    placed = (
        P("dp", None, "sp", None),
        P("dp", None, "sp", None),
        P("dp", None, "sp", None),
        P(("dp", "sp"), None),
        P(None, None, "dp"),
    )
    return jax.shard_map(
        on_device, mesh=mesh, in_specs=placed, out_specs=P("dp", "sp", None), check_vma=False
    )
```

profile of v0, /device:TPU:1, one launch (start us, length us, event | category | flops | bytes accessed | tf_op | source)
XLA Modules:
  0.0 269.0 jit_solution(7853102983301813299)
XLA Ops:
  6.5 3.2 %pad_maximum_fusion = bf16[32,64,768]{2,1,0:T(8,128)(2,1)} fusion(bf16[32,64,256]{2,1,0:T(8,128)(2,1)} %bitcast.74, bf16[32,64,256]{2,1,0:T(8,128)(2,1)} %bitcast.75, bf16[32,64,256]{2,1,0:T(8,128)(2,1)} %bitcast.76), kind=kLoop, calls=%fused_computation.6 | loop fusion | flops 9437184 | bytes 6291456 | tf_op jit(solution)/shard_map/concatenate | solution.py:10
  9.8 13.8 %all-to-all-start = ((bf16[32,64,768]{2,1,0:T(8,128)(2,1)}), bf16[32,64,768]{2,1,0:T(8,128)(2,1)S(1)}, u32[]{:S(2)}, u32[]{:S(2)}) async-start(bf16[32,64,768]{2,1,0:T(8,128)(2,1)} %pad_maximum_fusion), calls=%async_computation | async-start | bytes 6291456 | tf_op jit(solution)/shard_map/all_to_all | solution.py:12
  23.7 0.7 all-gather.2.cloned.1.call-update
  26.2 67.7 %all-to-all-done = bf16[32,64,768]{2,1,0:T(8,128)(2,1)S(1)} async-done(((bf16[32,64,768]{2,1,0:T(8,128)(2,1)}), bf16[32,64,768]{2,1,0:T(8,128)(2,1)S(1)}, u32[]{:S(2)}, u32[]{:S(2)}) %all-to-all-start) | async-done | bytes 3145760 | tf_op jit(solution)/shard_map/all_to_all | solution.py:12
  94.3 4.6 %subtract_convert_fusion.1 = (bf16[2048,128]{1,0:T(8,128)(2,1)S(1)}, bf16[2048,128]{1,0:T(8,128)(2,1)S(1)}, bf16[2048,128]{1,0:T(8,128)(2,1)S(1)}, bf16[2048,128]{1,0:T(8,128)(2,1)S(1)}) fusion(f32[2048,256]{1,0:T(8,128)S(1)} %get-tuple-element.85, f32[128]{0:T(128)S(1)} %multiply_power_fusion, f32[2048,256]{1,0:T(8,128)S(1)} %get-tuple-element.87), kind=kLoop, calls=%fused_computation.34 | loop fusion | flops 4456448 | bytes 6291968 | tf_op jit(solution)/shard_map/convert.10
  99.0 5.4 %fusion.13 = f32[32,256,256]{2,1,0:T(8,128)} fusion(bf16[32,64,256]{2,1,0:T(8,128)(2,1)S(1)} %bitcast.63, f32[32,64]{1,0:T(8,128)S(1)} %get-tuple-element.95, bf16[32,64,128]{2,1,0:T(8,128)(2,1)S(1)} %bitcast.69, bf16[32,64,128]{2,1,0:T(8,128)(2,1)S(1)} %bitcast.71), kind=kOutput, calls=%fused_computation.17 | convolution fusion | flops 271581184 | bytes 10493952 | tf_op jit(solution)/shard_map/while/body/eval_jaxpr/bmd,bme->bde/dot_general | solution.py:79
  104.3 97.5 %while.20 = (s32[]{:T(128)}, f32[256,256]{1,0:T(8,128)S(1)}, bf16[32,256,256]{2,1,0:T(8,128)(2,1)}, f32[32]{0:T(128)S(1)}, f32[32,256,256]{2,1,0:T(8,128)}, /*index=5*/s32[]{:T(128)}, s32[]{:T(128)}) while((s32[]{:T(128)}, f32[256,256]{1,0:T(8,128)S(1)}, bf16[32,256,256]{2,1,0:T(8,128)(2,1)}, f32[32]{0:T(128)S(1)}, ...), condition=%wide.region_2.3_spmd.clone, body=%wide.region_1.2_spmd.clone.sunk | while | flops 262147 | bytes 1180268 | solution.py:88
  105.7 1.7 bitcast_add_fusion.2
  108.7 1.7 bitcast_add_fusion.2
  111.7 1.7 bitcast_add_fusion.2
  114.8 1.7 bitcast_add_fusion.2
  117.8 1.7 bitcast_add_fusion.2
  120.9 1.7 bitcast_add_fusion.2
  123.9 1.7 bitcast_add_fusion.2
  127.0 1.7 bitcast_add_fusion.2
  130.0 1.7 bitcast_add_fusion.2
  131.7 0.7 fusion.40
  133.1 1.7 bitcast_add_fusion.2
  136.1 1.7 bitcast_add_fusion.2
  139.2 1.7 bitcast_add_fusion.2
  142.2 1.7 bitcast_add_fusion.2
  145.3 1.7 bitcast_add_fusion.2
  148.3 1.7 bitcast_add_fusion.2
  151.3 1.7 bitcast_add_fusion.2
  154.4 1.7 bitcast_add_fusion.2
  157.4 1.7 bitcast_add_fusion.2
  160.5 1.7 bitcast_add_fusion.2
  162.2 0.7 fusion.40
  163.6 1.7 bitcast_add_fusion.2
  166.6 1.7 bitcast_add_fusion.2
  168.3 0.7 fusion.40
  169.7 1.7 bitcast_add_fusion.2
  172.7 1.7 bitcast_add_fusion.2
  175.8 1.7 bitcast_add_fusion.2
  178.8 1.7 bitcast_add_fusion.2
  181.9 1.7 bitcast_add_fusion.2
  184.9 1.7 bitcast_add_fusion.2
  187.9 1.7 bitcast_add_fusion.2
  191.0 1.7 bitcast_add_fusion.2
  194.0 1.7 bitcast_add_fusion.2
  197.1 1.7 bitcast_add_fusion.2
  200.1 1.7 bitcast_add_fusion.2
  201.8 4.5 %fusion.25 = f32[32,64,256]{2,1,0:T(8,128)} fusion(bf16[32,256,256]{2,1,0:T(8,128)(2,1)} %get-tuple-element.56, bf16[32,64,128]{2,1,0:T(8,128)(2,1)S(1)} %bitcast.67, bf16[32,64,128]{2,1,0:T(8,128)(2,1)S(1)} %bitcast.65), kind=kOutput, calls=%fused_computation.38 | convolution fusion | flops 270532608 | bytes 7340032 | tf_op jit(solution)/shard_map/while/body/eval_jaxpr/bnd,bde->bne/dot_general | solution.py:92
  206.3 2.9 %fusion.11 = bf16[32,1,64,256]{3,2,0,1:T(8,128)(2,1)} fusion(f32[32,64,256]{2,1,0:T(8,128)} %fusion.25, bf16[32,64,256]{2,1,0:T(8,128)(2,1)S(1)} %bitcast.64, f32[32,64]{1,0:T(8,128)S(1)} %get-tuple-element.94, bf16[32,64,128]{2,1,0:T(8,128)(2,1)S(1)} %bitcast.70, bf16[32,64,128]{2,1,0:T(8,128)(2,1)S(1)} %bitcast.72, bf16[32,64,128]{2,1,0:T(8,128)(2,1)S(1)} %bitcast.68, ...), kind=kOutput, calls=%fused_computation.14 | convolution fusion | flops 140640256 | bytes 6311936 | tf_op jit(solution)/shard_map/while/body/eval_jaxpr/bnm,bme->bne/dot_general | solution.py:89
  209.2 1.3 slice_bitcast_fusion.3
  210.5 23.1 %all_to_all.22 = bf16[32,1,32,256]{3,2,1,0:T(8,128)(2,1)S(1)} all-to-all(bf16[32,1,32,256]{3,2,1,0:T(8,128)(2,1)S(1)} %get-tuple-element.92), channel_id=1, replica_groups=mesh['sp'=32,'dp'=16] {'sp'}, dimensions={0} | all-to-all | bytes 1048576 | tf_op jit(solution)/shard_map/all_to_all | solution.py:46
  233.6 21.2 %all_to_all.23 = bf16[32,1,32,256]{3,2,1,0:T(8,128)(2,1)S(1)} all-to-all(bf16[32,1,32,256]{3,2,1,0:T(8,128)(2,1)S(1)} %get-tuple-element.93), channel_id=1, replica_groups=mesh['sp'=32,'dp'=16] {'sp'}, dimensions={0} | all-to-all | bytes 1048576 | tf_op jit(solution)/shard_map/all_to_all | solution.py:46
  255.4 6.7 %fusion.7 = bf16[4,64,2048]{2,1,0:T(8,128)(2,1)} fusion(bf16[8,256,2048]{2,1,0:T(8,128)(2,1)} %all-gather.2.cloned.1.call-done, f32[4,8,64]{2,1,0:T(8,128)S(1)} %rsqrt_bitcast_fusion, f32[4,8,64,256]{3,2,1,0:T(8,128)S(1)} %bitcast.73), kind=kOutput, calls=%fused_computation.8 | convolution fusion | flops 2149056512 | bytes 11542528 | tf_op jit(solution)/shard_map/shtd,hde->ste/dot_general | solution.py:122
  (84 shorter events, 43.1 us)
Async XLA Ops:
  9.8 15.1 %copy-start.2 = (f32[1,2048]{1,0:T(1,128)S(1)}, f32[1,2048]{1,0:T(1,128)}, u32[]{:S(2)}) copy-start(f32[1,2048]{1,0:T(1,128)} %param.10) | copy-start | bytes 24580
  9.8 84.1 %all-to-all-start = ((bf16[32,64,768]{2,1,0:T(8,128)(2,1)}), bf16[32,64,768]{2,1,0:T(8,128)(2,1)S(1)}, u32[]{:S(2)}, u32[]{:S(2)}) async-start(bf16[32,64,768]{2,1,0:T(8,128)(2,1)} %pad_maximum_fusion), calls=%async_computation | async-start | bytes 6291456 | tf_op jit(solution)/shard_map/all_to_all | solution.py:12
  23.6 231.8 %all-gather.2.cloned.1.call-start = ((), (), s32[]{:S(2)}) async-start(), calls=%async_computation.3 | async-start | bytes 8912896 | tf_op jit(solution)/shard_map/all_gather | solution.py:100
  94.3 4.6 %copy-start = (bf16[1,2048,256]{2,1,0:T(8,128)(2,1)}, bf16[1,2048,256]{2,1,0:T(8,128)(2,1)S(1)}, u32[]{:S(2)}) copy-start(bf16[1,2048,256]{2,1,0:T(8,128)(2,1)S(1)} %get-tuple-element.86) | copy-start | bytes 3145732
  201.8 4.5 %copy-start.1 = (bf16[1,2048,256]{2,1,0:T(8,128)(2,1)S(1)}, bf16[1,2048,256]{2,1,0:T(8,128)(2,1)}, u32[]{:S(2)}) copy-start(bf16[1,2048,256]{2,1,0:T(8,128)(2,1)} %copy-done) | copy-start | bytes 3145732
Sparse Core Ops, SparseCore 0:
  26.5 70.5 all-gather.1
where the time goes:
time: 273 us; the launch traced here: 269 us
  other arithmetic  85.8 us (31%)
  waiting for transfers between devices  68.4 us (25%)
  blocking collectives  44.3 us (16%)
  local copies, waits for them, and re-layouts  23 us (8%)
  matrix products  19.5 us (7%)
  starting transfers between devices  13.9 us (5%)
  between operations  13.5 us (5%)
    all_to_all x1, waiting for transfers between devices, in_one_piece(): lax.all_to_all(both, axis, split_axis=split_dim, concat_axis=concat_dim,...  67.7 us
    add x32, other arithmetic, advance(): return (factor * state_now + update, state_now.astype(jnp.bfloat16))  54.5 us
    all_to_all x2, blocking collectives, several_exchanges(): lax.all_to_all(slab, axis, split_axis=0, concat_axis=0, tiled=True)  44.3 us
    dynamic_update_slice x32, other arithmetic, retain(): _, before = lax.scan(advance, start_state, (jnp.exp(ending[:, 0]), updates))  21.4 us
    dynamic_slice x32, local copies, waits for them, and re-layouts, retain(): _, before = lax.scan(advance, start_state, (jnp.exp(ending[:, 0]), updates))  20.9 us
    all_to_all x1, starting transfers between devices, in_one_piece(): lax.all_to_all(both, axis, split_axis=split_dim, concat_axis=concat_dim,...  13.8 us
    dot_general x1, matrix products, on_device(): jnp.einsum('shtd,hde->ste', normed, whole_w, preferred_element_type=jnp.f...  6.73 us
  transfers between devices with their start and end apart: 2, of which 1 were waited for; matrix products, arithmetic and copies ran while one was open for 44% of the time, Pallas kernels for 0%

commit v1 on v0

v1 whole, which is shorter than its diff:
```python
import functools

import jax
import jax.numpy as jnp
import numpy as np
from jax import lax
from jax.experimental import pallas as pl
from jax.experimental.pallas import tpu as pltpu
from jax.sharding import PartitionSpec as P

RING_X = 4
LANES = 128
MESH = pl.DeviceIdType.MESH
F32 = jnp.float32
BF16 = jnp.bfloat16


def take(ref, sem):
    pltpu.make_async_copy(ref, ref, sem).wait()


def kernel(
    dims,
    q_hbm, k_hbm, v_hbm, ld_hbm, w_hbm, freq_ref,
    out_ref,
    kv, qb, ldb, cosb, sinb, wrow, wcol, upd, s_in, s_out, o_snd, o_rcv, wb, acc,
    loc_w, ld_s, ld_r, kv_s, kv_r, q_s, q_r, ch_s, ch_r, o_s, o_r,
    wr_s, wr_r, wl_s, wl_r, p_s, p_r,
):
    X, Z, Y, G, J, T, D = dims
    N, L, HD = G * J, X * T, X * J * D
    R = Y // 2
    HALF = HD // 2
    sp, dp = lax.axis_index("sp"), lax.axis_index("dp")
    z, x = sp // X, sp % X
    y, c = dp // 2, dp % 2

    def at_x(d):
        return z * X + (x + d) % X

    def dp_of(yy):
        return ((yy + 2 * Y) % Y) * 2 + c

    right, left = dp_of(y + 1), dp_of(y - 1)
    mate = y * 2 + (1 - c)

    barrier = pltpu.get_barrier_semaphore()
    for d in range(1, X):
        pl.semaphore_signal(barrier, inc=1, device_id={"sp": at_x(d)}, device_id_type=MESH)
    for d in range(1, Z):
        pl.semaphore_signal(
            barrier, inc=1, device_id={"sp": ((z + d) % Z) * X + x}, device_id_type=MESH
        )
    for t in (right, left, mate):
        pl.semaphore_signal(barrier, inc=1, device_id={"dp": t}, device_id_type=MESH)
    pl.semaphore_wait(barrier, X + Z + 1)

    def remote(src, dst, ss, rs, **to):
        return pltpu.make_async_remote_copy(
            src_ref=src, dst_ref=dst, send_sem=ss, recv_sem=rs, device_id=to, device_id_type=MESH
        )

    for d in range(1, Z):
        to = (z + d) % Z
        remote(
            ld_hbm.at[:, pl.ds(to * L, L)], ldb.at[z], ld_s.at[d], ld_r.at[z], sp=to * X + x
        ).start()
    pltpu.make_async_copy(ld_hbm.at[:, pl.ds(z * L, L)], ldb.at[z], ld_r.at[z]).start()

    def send_rows(n, hbm, dst, ss, rs):
        s, j = n % G, n // G
        for d in (2, 1, 3) if X == 4 else range(1, X):
            to = (x + d) % X
            remote(hbm.at[s, to + X * j], dst, ss, rs, sp=z * X + to).start()
        pltpu.make_async_copy(hbm.at[s, x + X * j], dst, rs).start()

    @pl.loop(0, N)
    def _(n):
        mine = pl.ds(x * T, T)
        send_rows(n, k_hbm, kv.at[n, 0, mine], kv_s.at[n], kv_r.at[n])
        send_rows(n, v_hbm, kv.at[n, 1, mine], kv_s.at[n], kv_r.at[n])

    def ring_piece(k, sign):
        if k < R - 1:
            return pl.ds(0, HD)
        return pl.ds(0, HALF) if sign > 0 else pl.ds(HALF, HALF)

    def ring_send(k, sign):
        shard = dp_of(y - sign * k)
        rows = ring_piece(k, sign)
        src = w_hbm.at[rows] if k == 0 else wb.at[shard, rows]
        ss, rs = (wr_s, wr_r) if sign > 0 else (wl_s, wl_r)
        return remote(
            src, wb.at[shard, rows], ss.at[k], rs.at[k], dp=right if sign > 0 else left
        )

    def ring_recv(k, sign):
        shard = dp_of(y - sign * (k + 1))
        rs = wr_r if sign > 0 else wl_r
        take(wb.at[shard, ring_piece(k, sign)], rs.at[k])

    def to_mate(yy):
        shard = dp_of(yy)
        return remote(wb.at[shard], wb.at[shard], p_s.at[shard // 2], p_r.at[shard // 2], dp=mate)

    for sign in (1, -1):
        ring_send(0, sign).start()
    own_w = pltpu.make_async_copy(w_hbm, wb.at[dp], loc_w)
    own_w.start()
    remote(w_hbm, wb.at[dp], p_s.at[y], p_r.at[y], dp=mate).start()

    @pl.loop(0, N)
    def _(n):
        send_rows(n, q_hbm, qb.at[n, pl.ds(x * T, T)], q_s.at[n], q_r.at[n])

    @pl.when(z == 0)
    def _():
        s_in[...] = jnp.zeros_like(s_in)

    pos = (lax.broadcasted_iota(jnp.int32, (L, LANES), 0) + z * L).astype(F32)
    angle = pos * freq_ref[0:1, :]
    cosb[...] = jnp.cos(angle)
    sinb[...] = jnp.sin(angle)

    for i in range(Z):
        take(ldb.at[i], ld_r.at[i])
    run = jnp.concatenate([ldb[i] for i in range(Z)], axis=0)
    lane = lax.broadcasted_iota(jnp.int32, (Z, L), 1)
    step = 1
    while step < L:
        run = run + jnp.where(lane >= step, pltpu.roll(run, step, 1), 0.0)
        step *= 2
    cols = jnp.transpose(run)
    for i in range(Z):
        wrow[i] = run[i : i + 1]
        wcol[i] = jnp.broadcast_to(cols[:, i : i + 1], (L, LANES))

    def decay_row(n):
        return J * (n % G) + n // G

    def rotate(block):
        a, b = block[:, :LANES].astype(F32), block[:, LANES:].astype(F32)
        co, si = cosb[...], sinb[...]
        return (a * co - b * si).astype(BF16), (b * co + a * si).astype(BF16)

    def keys_in(n):
        i = decay_row(n)
        take(kv.at[n], kv_r.at[n])
        a, b = rotate(kv[n, 0])
        kv[n, 0, :, :LANES] = a
        kv[n, 0, :, LANES:] = b
        scale = jnp.exp(wcol[i, L - 1 : L, :] - wcol[i])
        scaled = jnp.concatenate(
            [(a.astype(F32) * scale).astype(BF16), (b.astype(F32) * scale).astype(BF16)], axis=1
        )
        got = lax.dot_general(
            scaled, kv[n, 1], (((0,), (0,)), ((), ())), preferred_element_type=F32
        )
        upd[n, 0] = got[:, :LANES]
        upd[n, 1] = got[:, LANES:]

    def chain_copy(n, hf):
        return remote(
            s_out.at[n, hf], s_in.at[n, hf], ch_s.at[n, hf], ch_r.at[n, hf],
            sp=jnp.minimum(z + 1, Z - 1) * X + x,
        )

    def chain(n):
        i = decay_row(n)
        factor = jnp.exp(wcol[i, L - 1 : L, :])
        for hf in range(2):
            @pl.when(z > 0)
            def _():
                take(s_in.at[n, hf], ch_r.at[n, hf])

            @pl.when(z < Z - 1)
            def _():
                s_out[n, hf] = (factor * s_in[n, hf].astype(F32) + upd[n, hf]).astype(BF16)
                chain_copy(n, hf).start()

    def outputs(n):
        i = decay_row(n)
        s, j = n % G, n // G
        take(qb.at[n], q_r.at[n])
        query = jnp.concatenate(rotate(qb[n]), axis=1)
        key, val = kv[n, 0], kv[n, 1]
        scores = lax.dot_general(
            query, key, (((1,), (1,)), ((), ())), preferred_element_type=F32
        )
        parts = []
        for m in range(L // LANES):
            lanes = slice(m * LANES, (m + 1) * LANES)
            spread = wcol[i] - wrow[i, :, lanes]
            causal = (
                lax.broadcasted_iota(jnp.int32, (L, LANES), 0)
                >= lax.broadcasted_iota(jnp.int32, (L, LANES), 1) + m * LANES
            )
            mask = jnp.where(causal, jnp.exp(jnp.where(causal, spread, 0.0)), 0.0)
            parts.append((scores[:, lanes] * mask).astype(BF16))
        weights = jnp.concatenate(parts, axis=1)
        local = jnp.dot(weights, val, preferred_element_type=F32)
        grow = jnp.exp(wcol[i])
        state = jnp.concatenate([s_in[n, 0], s_in[n, 1]], axis=1)
        carried = jnp.dot(query, state, preferred_element_type=F32)
        both = []
        for hf in range(2):
            lanes = slice(hf * LANES, (hf + 1) * LANES)
            both.append((local[:, lanes] + grow * carried[:, lanes]).astype(BF16).astype(F32))
        square = jnp.sum(both[0] * both[0] + both[1] * both[1], axis=1, keepdims=True)
        inv = lax.rsqrt(square * (1.0 / D) + 1e-6)
        o_snd[n, :, :LANES] = (both[0] * inv).astype(BF16)
        o_snd[n, :, LANES:] = (both[1] * inv).astype(BF16)
        rows = pl.ds(s * T, T)
        for d in (2, 1, 3) if X == 4 else range(1, X):
            to = (x + d) % X
            remote(
                o_snd.at[n, pl.ds(to * T, T)], o_rcv.at[j, x, rows], o_s.at[n], o_r.at[j, x],
                sp=z * X + to,
            ).start()
        o_rcv[j, x, rows, :] = o_snd[n, pl.ds(x * T, T), :]

    def ring_step(k):
        for sign in (1, -1):
            ring_recv(k - 1, sign)
            if k < R:
                ring_send(k, sign).start()
        if k < R:
            to_mate(y - k).start()
            to_mate(y + k).start()
        else:
            to_mate(y + R).start()

    lag = Z - 1 - z
    due = {k: jnp.maximum(4 * k + k // 3 - (6 * z + 4) // 5, 0) for k in range(1, R)}

    @pl.loop(0, N + Z - 1)
    def _(t):
        for k in range(1, R):
            @pl.when(t == due[k])
            def _(k=k):
                ring_step(k)

        @pl.when(t < N)
        def _():
            n = jnp.minimum(t, N - 1)
            keys_in(n)
            chain(n)

        @pl.when((t >= lag) & (t < lag + N))
        def _():
            outputs(jnp.clip(t - lag, 0, N - 1))

    ring_step(R)
    own_w.wait()
    for yy in range(Y):
        take(wb.at[2 * yy], p_r.at[yy])

    def project(j, yy):
        total = None
        for h in range(X):
            rows = slice((h + X * j) * D, (h + X * j + 1) * D)
            w_pair = jnp.concatenate([wb[2 * yy, rows, :], wb[2 * yy + 1, rows, :]], axis=1)
            term = jnp.dot(o_rcv[j, h], w_pair, preferred_element_type=F32)
            total = term if total is None else total + term
        return total

    for j in range(J):
        for d in range(1, X):
            src = (x + d) % X
            take(o_rcv.at[j, src], o_r.at[j, src])

        @pl.loop(0, Y)
        def _(yy):
            total = project(j, yy)
            if j > 0:
                total = total + acc[yy]
            if j < J - 1:
                acc[yy] = total
            else:
                cols2 = pl.ds(pl.multiple_of(yy * 2 * LANES, 2 * LANES), 2 * LANES)
                out_ref[:, cols2] = total.astype(BF16)

    for d in range(1, Z):
        take(ldb.at[0], ld_s.at[d])

    @pl.loop(0, N)
    def _(n):
        gone = pl.ds(0, (X - 1) * T)
        take(kv.at[n, :, gone], kv_s.at[n])
        take(qb.at[n, gone], q_s.at[n])
        take(qb.at[n, gone], o_s.at[n])

        @pl.when(z < Z - 1)
        def _():
            for hf in range(2):
                take(s_out.at[n, hf], ch_s.at[n, hf])

    for k in range(R):
        take(wb.at[0, ring_piece(k, 1)], wr_s.at[k])
        take(wb.at[0, ring_piece(k, -1)], wl_s.at[k])
    for yy in range(Y):
        take(wb.at[0], p_s.at[yy])


def on_device(queries, keys, values, log_decay, w_out):
    G, H, T, D = queries.shape
    X = RING_X
    Z = lax.axis_size("sp") // X
    Y = lax.axis_size("dp") // 2
    J = H // X
    N, L, HD = G * J, X * T, H * D
    F = w_out.shape[2]
    W = F * 2 * Y
    R = Y // 2
    assert N == Z and D == 2 * LANES and F == LANES and L == 2 * LANES
    half = D // 2
    freq = jnp.asarray(
        np.power(10000.0, -np.arange(half, dtype=np.float64) / half).astype(np.float32)
    ).reshape(1, half)
    dma = pltpu.SemaphoreType.DMA
    anyspace = pl.BlockSpec(memory_space=pl.ANY)
    vmem = pl.BlockSpec(memory_space=pltpu.VMEM)
    out = pl.pallas_call(
        functools.partial(kernel, (X, Z, Y, G, J, T, D)),
        out_shape=jax.ShapeDtypeStruct((G * T, W), BF16),
        in_specs=[anyspace] * 5 + [vmem],
        out_specs=vmem,
        scratch_shapes=[
            pltpu.VMEM((N, 2, L, D), BF16),
            pltpu.VMEM((N, L, D), BF16),
            pltpu.VMEM((Z, 1, L), F32),
            pltpu.VMEM((L, LANES), F32),
            pltpu.VMEM((L, LANES), F32),
            pltpu.VMEM((Z, 1, L), F32),
            pltpu.VMEM((Z, L, LANES), F32),
            pltpu.VMEM((N, 2, D, LANES), F32),
            pltpu.VMEM((N, 2, D, LANES), BF16),
            pltpu.VMEM((N, 2, D, LANES), BF16),
            pltpu.VMEM((N, L, D), BF16),
            pltpu.VMEM((J, X, G * T, D), BF16),
            pltpu.VMEM((2 * Y, HD, F), BF16),
            pltpu.VMEM((Y, G * T, 2 * F), F32),
            dma,
            dma((Z,)), dma((Z,)),
            dma((N,)), dma((N,)),
            dma((N,)), dma((N,)),
            dma((N, 2)), dma((N, 2)),
            dma((N,)), dma((J, X)),
            dma((R,)), dma((R,)), dma((R,)), dma((R,)),
            dma((Y,)), dma((Y,)),
        ],
        compiler_params=pltpu.CompilerParams(
            collective_id=0, has_side_effects=True, vmem_limit_bytes=48 * 1024 * 1024
        ),
        name="retention",
    )(queries, keys, values, log_decay, w_out.reshape(HD, F), freq)
    return out.reshape(G, T, W)


def solution(mesh):
    placed = (
        P("dp", None, "sp", None),
        P("dp", None, "sp", None),
        P("dp", None, "sp", None),
        P(("dp", "sp"), None),
        P(None, None, "dp"),
    )
    return jax.shard_map(
        on_device, mesh=mesh, in_specs=placed, out_specs=P("dp", "sp", None), check_vma=False
    )
```

time: 273 us -> 74.9 us (0.27); the launches traced: 269 us -> 74.6 us
  other arithmetic: 85.8 us -> 0 us
  waiting for transfers between devices: 68.4 us -> 0 us
  Pallas kernels: 0 us -> 67.5 us
  blocking collectives: 44.3 us -> 0 us
  matrix products: 19.5 us -> 0 us
  local copies, waits for them, and re-layouts: 23 us -> 7.04 us
  starting transfers between devices: 13.9 us -> 0 us
  between operations: 13.5 us -> 0.02 us
    all_to_all x1 -> x0, waiting for transfers between devices: 67.7 us -> none  [in_one_piece(): lax.all_to_all(both, axis, split_axis=split_dim, concat_axis=concat_dim,...]
    pallas_call x0 -> x1, Pallas kernels: none -> 67.5 us  [on_device(): pl.pallas_call(functools.partial(kernel, (X, Z, Y, G, J, T, D)), out_shap...]
    add x32 -> x0, other arithmetic: 54.5 us -> none  [advance(): return (factor * state_now + update, state_now.astype(jnp.bfloat16))]
    all_to_all x2 -> x0, blocking collectives: 44.3 us -> none  [several_exchanges(): lax.all_to_all(slab, axis, split_axis=0, concat_axis=0, tiled=True)]
    dynamic_update_slice x32 -> x0, other arithmetic: 21.4 us -> none  [retain(): _, before = lax.scan(advance, start_state, (jnp.exp(ending[:, 0]), updates))]
    dynamic_slice x32 -> x0, local copies, waits for them, and re-layouts: 20.9 us -> none  [retain(): _, before = lax.scan(advance, start_state, (jnp.exp(ending[:, 0]), updates))]
    dot_general x4 -> x0, matrix products: 19.5 us -> none  [the longest x1 6.73 us: on_device(): jnp.einsum('shtd,hde->ste', normed, whole_w, preferred_element_type=jnp.f...]
    all_to_all x1 -> x0, starting transfers between devices: 13.8 us -> none  [in_one_piece(): lax.all_to_all(both, axis, split_axis=split_dim, concat_axis=concat_dim,...]
  transfers between devices with their start and end apart: 2 -> 0, of which waited for: 1 -> 0; matrix products, arithmetic and copies ran while one was open for 44% -> 0% of each run, Pallas kernels for 0% -> 0%
where the time goes in v1:
time: 74.9 us; the launch traced here: 74.6 us
  Pallas kernels  67.5 us (90%)
  local copies, waits for them, and re-layouts  7.04 us (9%)
    pallas_call x1, Pallas kernels, on_device(): pl.pallas_call(functools.partial(kernel, (X, Z, Y, G, J, T, D)), out_shap...  67.5 us
    unnamed x13, local copies, waits for them, and re-layouts  7.04 us

profile of v1, /device:TPU:1, one launch (start us, length us, event | category | flops | bytes accessed | tf_op | source)
XLA Modules:
  0.0 74.6 jit_solution(8305645208187918335)
XLA Ops:
  0.0 0.0 copy-start.5
  0.0 0.7 copy-done.5
  0.7 0.0 copy-start
  0.7 1.2 %copy-done = bf16[4,8,64,256]{3,2,1,0:T(8,128)(2,1)S(1)} copy-done((bf16[4,8,64,256]{3,2,1,0:T(8,128)(2,1)S(1)}, bf16[4,8,64,256]{3,2,1,0:T(8,128)(2,1)}, u32[]{:S(2)}) %copy-start) | copy-done | bytes 1048600
  1.9 0.0 copy-start.1
  1.9 1.2 %copy-done.1 = bf16[4,8,64,256]{3,2,1,0:T(8,128)(2,1)S(1)} copy-done((bf16[4,8,64,256]{3,2,1,0:T(8,128)(2,1)S(1)}, bf16[4,8,64,256]{3,2,1,0:T(8,128)(2,1)}, u32[]{:S(2)}) %copy-start.1) | copy-done | bytes 1048600
  3.1 0.0 copy-start.2
  3.1 1.2 %copy-done.2 = bf16[4,8,64,256]{3,2,1,0:T(8,128)(2,1)S(1)} copy-done((bf16[4,8,64,256]{3,2,1,0:T(8,128)(2,1)S(1)}, bf16[4,8,64,256]{3,2,1,0:T(8,128)(2,1)}, u32[]{:S(2)}) %copy-start.2) | copy-done | bytes 1048600
  4.3 0.0 copy-start.3
  4.3 1.0 %copy-done.3 = bf16[8,256,128]{2,1,0:T(8,128)(2,1)S(1)} copy-done((bf16[8,256,128]{2,1,0:T(8,128)(2,1)S(1)}, bf16[8,256,128]{2,1,0:T(8,128)(2,1)}, u32[]{:S(2)}) %copy-start.3) | copy-done | bytes 524312
  5.4 0.0 copy-start.4
  5.4 0.7 copy-done.4
  6.1 67.5 %retention.1 = bf16[256,2048]{1,0:T(8,128)(2,1)S(1)} custom-call(bf16[4,8,64,256]{3,2,1,0:T(8,128)(2,1)S(1)} %copy-done, bf16[4,8,64,256]{3,2,1,0:T(8,128)(2,1)S(1)} %copy-done.1, bf16[4,8,64,256]{3,2,1,0:T(8,128)(2,1)S(1)} %copy-done.2, f32[1,2048]{1,0:T(1,128)S(1)} %copy-done.4, bf16[2048,128]{1,0:T(8,128)(2,1)S(1)} %bitcast.3, f32[1,128]{1,0:T(1,128)S(1)} %copy-done.5), custom_call_target="tpu_custom_call" | custom-call | tf_op jit(solution)/shard_map/retention/pallas_call | solution.py:323
  73.6 1.0 %copy.8 = bf16[4,64,2048]{2,1,0:T(8,128)(2,1)} copy(bf16[4,64,2048]{2,1,0:T(8,128)(2,1)S(1)} %bitcast.2) | data formatting | bytes 2097152
Async XLA Ops:
  0.0 0.7 copy-start.5
  0.7 1.2 %copy-start = (bf16[4,8,64,256]{3,2,1,0:T(8,128)(2,1)S(1)}, bf16[4,8,64,256]{3,2,1,0:T(8,128)(2,1)}, u32[]{:S(2)}) copy-start(bf16[4,8,64,256]{3,2,1,0:T(8,128)(2,1)} %q_hbm.1) | copy-start | bytes 3145732
  1.9 1.2 %copy-start.1 = (bf16[4,8,64,256]{3,2,1,0:T(8,128)(2,1)S(1)}, bf16[4,8,64,256]{3,2,1,0:T(8,128)(2,1)}, u32[]{:S(2)}) copy-start(bf16[4,8,64,256]{3,2,1,0:T(8,128)(2,1)} %k_hbm.1) | copy-start | bytes 3145732
  3.1 1.2 %copy-start.2 = (bf16[4,8,64,256]{3,2,1,0:T(8,128)(2,1)S(1)}, bf16[4,8,64,256]{3,2,1,0:T(8,128)(2,1)}, u32[]{:S(2)}) copy-start(bf16[4,8,64,256]{3,2,1,0:T(8,128)(2,1)} %v_hbm.1) | copy-start | bytes 3145732
  4.3 1.0 %copy-start.3 = (bf16[8,256,128]{2,1,0:T(8,128)(2,1)S(1)}, bf16[8,256,128]{2,1,0:T(8,128)(2,1)}, u32[]{:S(2)}) copy-start(bf16[8,256,128]{2,1,0:T(8,128)(2,1)} %param.10) | copy-start | bytes 1572868
  5.4 0.7 copy-start.4

commit v2 on v1

v2 whole, which is shorter than its diff:
```python
import functools

import jax
import jax.numpy as jnp
import numpy as np
from jax import lax
from jax.experimental import pallas as pl
from jax.experimental.pallas import tpu as pltpu
from jax.sharding import PartitionSpec as P

RING_X = 4
PIECES = 4
LANES = 128
MESH = pl.DeviceIdType.MESH
F32 = jnp.float32
BF16 = jnp.bfloat16


def take(ref, sem):
    pltpu.make_async_copy(ref, ref, sem).wait()


def kernel(
    dims,
    q_hbm, k_hbm, v_hbm, ld_hbm, w_hbm, freq_hbm,
    out_ref,
    kv, qb, ldb, cosb, sinb, wrow, wcol, upd, s_in, s_out, loc, o_snd, o_rcv, wb, acc, freq_ref,
    loc_f, loc_w, loc_d, loc_x, dr_s, dr_r, kv_s, kv_r, q_s, q_r, ch_s, ch_r, o_s, o_r,
    wr_s, wr_r, wl_s, wl_r, p_s, p_r,
):
    X, Z, Y, G, J, T, D = dims
    N, L, HD = G * J, X * T, X * J * D
    R = Y // 2
    HALF = HD // 2
    ROWS = D // PIECES
    sp, dp = lax.axis_index("sp"), lax.axis_index("dp")
    z, x = sp // X, sp % X
    y, c = dp // 2, dp % 2

    def dp_of(yy):
        return ((yy + 2 * Y) % Y) * 2 + c

    def sp_of(zz):
        return ((zz + Z) % Z) * X + x

    right, left, mate = dp_of(y + 1), dp_of(y - 1), y * 2 + (1 - c)
    up, down = sp_of(z + 1), sp_of(z - 1)
    partners = [{"sp": z * X + (x + d) % X} for d in range(1, X)] + [{"dp": right}, {"dp": left}]
    others = [{"sp": sp_of(z + d)} for d in range(1, Z)] + [{"dp": mate}]

    def remote(src, dst, ss, rs, **to):
        return pltpu.make_async_remote_copy(
            src_ref=src, dst_ref=dst, send_sem=ss, recv_sem=rs, device_id=to, device_id_type=MESH
        )

    freq_in = pltpu.make_async_copy(freq_hbm, freq_ref, loc_f)
    freq_in.start()
    own_w = pltpu.make_async_copy(w_hbm, wb.at[dp], loc_w)
    own_w.start()
    own_d = pltpu.make_async_copy(ld_hbm, ldb.at[z], loc_d)
    own_d.start()

    barrier = pltpu.get_barrier_semaphore()
    for to in partners + others:
        pl.semaphore_signal(barrier, inc=1, device_id=to, device_id_type=MESH)
    pl.semaphore_wait(barrier, len(partners) + len(others))

    def half(k, sign):
        first = (k % 2 == 0) == (sign > 0)
        return pl.ds(0, HALF) if first else pl.ds(HALF, HALF)

    def ring_send(k, sign):
        shard = dp_of(y - sign * (k // 2))
        rows = half(k, sign)
        src = w_hbm.at[rows] if k < 2 else wb.at[shard, rows]
        ss, rs = (wr_s, wr_r) if sign > 0 else (wl_s, wl_r)
        return remote(
            src, wb.at[shard, rows], ss.at[k], rs.at[k], dp=right if sign > 0 else left
        )

    def ring_step(k):
        for sign in (1, -1):
            shard = dp_of(y - sign * (k // 2 + 1))
            rows = half(k, sign)
            take(wb.at[shard, rows], (wr_r if sign > 0 else wl_r).at[k])
            if k + 2 < 2 * R - 1:
                ring_send(k + 2, sign).start()
            remote(
                wb.at[shard, rows], wb.at[shard, rows], p_s.at[shard // 2], p_r.at[shard // 2], dp=mate
            ).start()

    for k in range(min(2, 2 * R - 1)):
        for sign in (1, -1):
            ring_send(k, sign).start()

    mine = pl.ds(x * T, T)
    targets = [(x + d) % X for d in ((2, 1, 3) if X == 4 else range(1, X))]
    for n in range(N):
        heads, g = X * (n // G), n % G
        for m, hbm in enumerate((k_hbm, v_hbm)):
            for to in targets:
                remote(
                    hbm.at[g, to + heads], kv.at[n, m, mine], kv_s.at[n], kv_r.at[n], sp=z * X + to
                ).start()
    stay = []
    for j in range(J):
        items = pl.ds(j * G, G)
        for m, hbm in enumerate((k_hbm, v_hbm, q_hbm)):
            dst = qb.at[items, mine] if m == 2 else kv.at[items, m, mine]
            stay.append(pltpu.make_async_copy(hbm.at[:, x + X * j], dst, loc_x.at[j, m]))
            stay[-1].start()


    for d in range(1, Z):
        to = (z + d) % Z
        remote(ld_hbm, ldb.at[z], dr_s.at[d], dr_r.at[z], sp=to * X + x).start()
    remote(w_hbm, wb.at[dp], p_s.at[y], p_r.at[y], dp=mate).start()

    for j in range(J):
        for to in targets:
            remote(
                q_hbm.at[:, to + X * j], qb.at[pl.ds(j * G, G), mine], q_s.at[j], q_r.at[j],
                sp=z * X + to,
            ).start()

    @pl.when(z == 0)
    def _():
        s_in[...] = jnp.zeros_like(s_in)

    pos = (lax.broadcasted_iota(jnp.int32, (L, LANES), 0) + z * L).astype(F32)
    freq_in.wait()
    angle = pos * freq_ref[0:1, :]
    cosb[...] = jnp.cos(angle)
    sinb[...] = jnp.sin(angle)

    for d in range(1, Z):
        take(ldb.at[(z + d) % Z], dr_r.at[(z + d) % Z])
    own_d.wait()
    for copy in stay:
        copy.wait()

    here = pl.ds(pl.multiple_of(z * L, L), L)
    run = jnp.concatenate([ldb[i, :, here] for i in range(Z)], axis=0)
    lane = lax.broadcasted_iota(jnp.int32, (Z, L), 1)
    step = 1
    while step < L:
        run = run + jnp.where(lane >= step, pltpu.roll(run, step, 1), 0.0)
        step *= 2
    cols = jnp.transpose(run)
    for i in range(Z):
        wrow[i] = run[i : i + 1]
        wcol[i] = jnp.broadcast_to(cols[:, i : i + 1], (L, LANES))

    def decay_row(n):
        return J * (n % G) + n // G

    def rotate(block):
        a, b = block[:, :LANES].astype(F32), block[:, LANES:].astype(F32)
        co, si = cosb[...], sinb[...]
        return (a * co - b * si).astype(BF16), (b * co + a * si).astype(BF16)

    def keys_in(n):
        i = decay_row(n)
        take(kv.at[n, :, pl.ds(0, (X - 1) * T)], kv_r.at[n])
        a, b = rotate(kv[n, 0])
        kv[n, 0, :, :LANES] = a
        kv[n, 0, :, LANES:] = b
        scale = jnp.exp(wcol[i, L - 1 : L, :] - wcol[i])
        scaled = jnp.concatenate(
            [(a.astype(F32) * scale).astype(BF16), (b.astype(F32) * scale).astype(BF16)], axis=1
        )
        upd[n] = lax.dot_general(
            scaled, kv[n, 1], (((0,), (0,)), ((), ())), preferred_element_type=F32
        )

    def chain(n):
        factor = jnp.exp(wcol[decay_row(n), L - 1 : L, :])
        factor = jnp.concatenate([factor, factor], axis=1)
        for p in range(PIECES):
            rows = pl.ds(p * ROWS, ROWS)

            @pl.when(z > 0)
            def _():
                take(s_in.at[n, rows], ch_r.at[n, p])

            @pl.when(z < Z - 1)
            def _():
                s_out[n, rows, :] = (
                    factor * s_in[n, rows, :].astype(F32) + upd[n, rows, :]
                ).astype(BF16)
                remote(
                    s_out.at[n, rows], s_in.at[n, rows], ch_s.at[n, p], ch_r.at[n, p], sp=up
                ).start()

    def outputs_local(n):
        i = decay_row(n)

        @pl.when(n % G == 0)
        def _():
            take(qb.at[pl.ds(0, G), pl.ds(0, (X - 1) * T)], q_r.at[n // G])

        a, b = rotate(qb[n])
        qb[n, :, :LANES] = a
        qb[n, :, LANES:] = b
        scores = lax.dot_general(
            jnp.concatenate([a, b], axis=1), kv[n, 0], (((1,), (1,)), ((), ())),
            preferred_element_type=F32,
        )
        parts = []
        for m in range(L // LANES):
            lanes = slice(m * LANES, (m + 1) * LANES)
            spread = wcol[i] - wrow[i, :, lanes]
            causal = (
                lax.broadcasted_iota(jnp.int32, (L, LANES), 0)
                >= lax.broadcasted_iota(jnp.int32, (L, LANES), 1) + m * LANES
            )
            mask = jnp.where(causal, jnp.exp(jnp.where(causal, spread, 0.0)), 0.0)
            parts.append((scores[:, lanes] * mask).astype(BF16))
        weights = jnp.concatenate(parts, axis=1)
        loc[...] = jnp.dot(weights, kv[n, 1], preferred_element_type=F32)

    def outputs(n):
        s, j = n % G, n // G
        grow = jnp.exp(wcol[decay_row(n)])
        carried = jnp.dot(qb[n], s_in[n], preferred_element_type=F32)
        both = []
        for hf in range(2):
            lanes = slice(hf * LANES, (hf + 1) * LANES)
            both.append((loc[:, lanes] + grow * carried[:, lanes]).astype(BF16).astype(F32))
        square = jnp.sum(both[0] * both[0] + both[1] * both[1], axis=1, keepdims=True)
        inv = lax.rsqrt(square * (1.0 / D) + 1e-6)
        o_snd[n, :, :LANES] = (both[0] * inv).astype(BF16)
        o_snd[n, :, LANES:] = (both[1] * inv).astype(BF16)
        rows = pl.ds(s * T, T)
        for to in targets:
            remote(
                o_snd.at[n, pl.ds(to * T, T)], o_rcv.at[j, x, rows], o_s.at[n], o_r.at[j, x],
                sp=z * X + to,
            ).start()
        o_rcv[j, x, rows, :] = o_snd[n, pl.ds(x * T, T), :]

    lag = jnp.minimum(2 * (Z - 1 - z), N)
    last = N + Z

    def due(k):
        at = 18 + 20 * k - 9 * z
        late = 8 + jnp.maximum(at - 80, 0) // 5
        return jnp.clip(jnp.where(at > 80, late, at // 10), 0, last)

    @pl.loop(0, last + 1)
    def _(t):
        for k in range(2 * R - 1):
            @pl.when(t == due(k))
            def _(k=k):
                ring_step(k)

        n = jnp.clip(t - lag, 0, N - 1)
        leaving = (t >= lag) & (t < lag + N)

        @pl.when(t < N)
        def _():
            keys_in(jnp.minimum(t, N - 1))

        @pl.when(leaving)
        def _():
            outputs_local(n)

        @pl.when(t < N)
        def _():
            chain(jnp.minimum(t, N - 1))

        @pl.when(leaving)
        def _():
            outputs(n)

    own_w.wait()

    def project(j, yy):
        total = None
        for h in range(X):
            rows = slice((h + X * j) * D, (h + X * j + 1) * D)
            w_pair = jnp.concatenate([wb[2 * yy, rows, :], wb[2 * yy + 1, rows, :]], axis=1)
            term = jnp.dot(o_rcv[j, h], w_pair, preferred_element_type=F32)
            total = term if total is None else total + term
        return total

    for j in range(J):
        for d in range(1, X):
            src = (x + d) % X
            take(o_rcv.at[j, src], o_r.at[j, src])

        @pl.loop(0, Y)
        def _(k):
            yy = (y + Y + (1 - 2 * ((k + 1) % 2)) * ((k + 1) // 2)) % Y
            if j == 0:
                take(wb.at[0], p_r.at[yy])
            total = project(j, yy)
            if j > 0:
                total = total + acc[yy]
            if j < J - 1:
                acc[yy] = total
            else:
                cols2 = pl.ds(pl.multiple_of(yy * 2 * LANES, 2 * LANES), 2 * LANES)
                out_ref[:, cols2] = total.astype(BF16)

    for j in range(J):
        take(qb.at[pl.ds(0, G), pl.ds(0, (X - 1) * T)], q_s.at[j])
    for d in range(1, Z):
        take(ldb.at[0], dr_s.at[d])

    @pl.loop(0, N)
    def _(n):
        gone = pl.ds(0, (X - 1) * T)
        take(kv.at[n, :, gone], kv_s.at[n])
        take(qb.at[n, gone], o_s.at[n])

        @pl.when(z < Z - 1)
        def _():
            for p in range(PIECES):
                take(s_out.at[n, pl.ds(0, ROWS)], ch_s.at[n, p])

    for k in range(2 * R - 1):
        take(wb.at[0, pl.ds(0, HALF)], wr_s.at[k])
        take(wb.at[0, pl.ds(0, HALF)], wl_s.at[k])
    for yy in range(Y):
        take(wb.at[0], p_s.at[yy])


def on_device(queries, keys, values, log_decay, w_out):
    G, H, T, D = queries.shape
    X = RING_X
    Z = lax.axis_size("sp") // X
    Y = lax.axis_size("dp") // 2
    J = H // X
    N, L, HD = G * J, X * T, H * D
    F = w_out.shape[2]
    W = F * 2 * Y
    R = Y // 2
    assert N == Z and D == 2 * LANES and F == LANES and L == 2 * LANES
    half = D // 2
    freq = jnp.asarray(
        np.power(10000.0, -np.arange(half, dtype=np.float64) / half).astype(np.float32)
    ).reshape(1, half)
    dma = pltpu.SemaphoreType.DMA
    hbm = pl.BlockSpec(memory_space=pltpu.HBM)
    vmem = pl.BlockSpec(memory_space=pltpu.VMEM)
    out = pl.pallas_call(
        functools.partial(kernel, (X, Z, Y, G, J, T, D)),
        out_shape=jax.ShapeDtypeStruct((G * T, W), BF16),
        in_specs=[hbm] * 6,
        out_specs=vmem,
        scratch_shapes=[
            pltpu.VMEM((N, 2, L, D), BF16),
            pltpu.VMEM((N, L, D), BF16),
            pltpu.VMEM((Z, 1, Z * L), F32),
            pltpu.VMEM((L, LANES), F32),
            pltpu.VMEM((L, LANES), F32),
            pltpu.VMEM((Z, 1, L), F32),
            pltpu.VMEM((Z, L, LANES), F32),
            pltpu.VMEM((N, D, D), F32),
            pltpu.VMEM((N, D, D), BF16),
            pltpu.VMEM((N, D, D), BF16),
            pltpu.VMEM((L, D), F32),
            pltpu.VMEM((N, L, D), BF16),
            pltpu.VMEM((J, X, G * T, D), BF16),
            pltpu.VMEM((2 * Y, HD, F), BF16),
            pltpu.VMEM((Y, G * T, 2 * F), F32),
            pltpu.VMEM((1, LANES), F32),
            dma,
            dma,
            dma,
            dma((J, 3)),
            dma((Z,)), dma((Z,)),
            dma((N,)), dma((N,)),
            dma((J,)), dma((J,)),
            dma((N, PIECES)), dma((N, PIECES)),
            dma((N,)), dma((J, X)),
            dma((2 * R,)), dma((2 * R,)), dma((2 * R,)), dma((2 * R,)),
            dma((Y,)), dma((Y,)),
        ],
        compiler_params=pltpu.CompilerParams(
            collective_id=0, has_side_effects=True, vmem_limit_bytes=67043328
        ),
        name="retention",
    )(queries, keys, values, log_decay, w_out.reshape(HD, F), freq)
    return out.reshape(G, T, W)


def solution(mesh):
    placed = (
        P("dp", None, "sp", None),
        P("dp", None, "sp", None),
        P("dp", None, "sp", None),
        P(("dp", "sp"), None),
        P(None, None, "dp"),
    )
    return jax.shard_map(
        on_device, mesh=mesh, in_specs=placed, out_specs=P("dp", "sp", None), check_vma=False
    )
```

time: 74.9 us -> 68.2 us (0.911)
  the two profiles are of different devices: /device:TPU:1 before, /device:TPU:448 now
where the time goes in v2:
time: 68.2 us; the launch traced here: 68.1 us
  Pallas kernels  65.8 us (96%)
  local copies, waits for them, and re-layouts  2.3 us (3%)
    pallas_call x1, Pallas kernels, on_device(): pl.pallas_call(functools.partial(kernel, (X, Z, Y, G, J, T, D)), out_shap...  65.8 us
    unnamed x1, local copies, waits for them, and re-layouts  2.3 us

profile of v2, /device:TPU:448, one launch (start us, length us, event | category | flops | bytes accessed | tf_op | source)
XLA Modules:
  0.0 68.1 jit_solution(17151953034496101132)
XLA Ops:
  0.0 65.8 %retention.1 = bf16[256,2048]{1,0:T(8,128)(2,1)} custom-call(bf16[4,8,64,256]{3,2,1,0:T(8,128)(2,1)} %q_hbm.1, bf16[4,8,64,256]{3,2,1,0:T(8,128)(2,1)} %k_hbm.1, bf16[4,8,64,256]{3,2,1,0:T(8,128)(2,1)} %v_hbm.1, f32[1,2048]{1,0:T(1,128)} %ld_hbm.1, bf16[2048,128]{1,0:T(8,128)(2,1)} %bitcast.3, f32[1,128]{1,0:T(1,128)} %constant.7.freq_hbm), custom_call_target="tpu_custom_call" | custom-call | tf_op jit(solution)/shard_map/retention/pallas_call | solution.py:347
  65.8 2.3 %copy.8 = bf16[4,64,2048]{2,1,0:T(8,128)(2,1)} copy(bf16[4,64,2048]{2,1,0:T(8,128)(2,1)} %bitcast.2) | data formatting | bytes 2097152

commit v3 on v2

--- a/solution.py
+++ b/solution.py
@@ -24,7 +24,7 @@
     dims,
     q_hbm, k_hbm, v_hbm, ld_hbm, w_hbm, freq_hbm,
     out_ref,
-    kv, qb, ldb, cosb, sinb, wrow, wcol, upd, s_in, s_out, loc, o_snd, o_rcv, wb, acc, freq_ref,
+    kv, qb, own_row, ldb, cosb, sinb, wrow, wcol, upd, s_in, s_out, loc, o_snd, o_rcv, wb, acc, freq_ref,
     loc_f, loc_w, loc_d, loc_x, dr_s, dr_r, kv_s, kv_r, q_s, q_r, ch_s, ch_r, o_s, o_r,
     wr_s, wr_r, wl_s, wl_r, p_s, p_r,
 ):
@@ -45,8 +45,7 @@
 
     right, left, mate = dp_of(y + 1), dp_of(y - 1), y * 2 + (1 - c)
     up, down = sp_of(z + 1), sp_of(z - 1)
-    partners = [{"sp": z * X + (x + d) % X} for d in range(1, X)] + [{"dp": right}, {"dp": left}]
-    others = [{"sp": sp_of(z + d)} for d in range(1, Z)] + [{"dp": mate}]
+    partners = [{"sp": z * X + (x + d) % X} for d in range(1, X)] + [{"dp": right}, {"dp": left}, {"dp": mate}]
 
     def remote(src, dst, ss, rs, **to):
         return pltpu.make_async_remote_copy(
@@ -57,13 +56,19 @@
     freq_in.start()
     own_w = pltpu.make_async_copy(w_hbm, wb.at[dp], loc_w)
     own_w.start()
-    own_d = pltpu.make_async_copy(ld_hbm, ldb.at[z], loc_d)
+    own_d = pltpu.make_async_copy(ld_hbm, own_row, loc_d)
     own_d.start()
 
     barrier = pltpu.get_barrier_semaphore()
-    for to in partners + others:
+    for to in partners:
         pl.semaphore_signal(barrier, inc=1, device_id=to, device_id_type=MESH)
-    pl.semaphore_wait(barrier, len(partners) + len(others))
+    for d in range(1, Z):
+
+        @pl.when((z + d) % Z != 0)
+        def _():
+            pl.semaphore_signal(barrier, inc=1, device_id={"sp": sp_of(z + d)}, device_id_type=MESH)
+
+    pl.semaphore_wait(barrier, len(partners) + jnp.where(z == 0, 0, Z - 1))
 
     def half(k, sign):
         first = (k % 2 == 0) == (sign > 0)
@@ -89,37 +94,48 @@
                 wb.at[shard, rows], wb.at[shard, rows], p_s.at[shard // 2], p_r.at[shard // 2], dp=mate
             ).start()
 
-    for k in range(min(2, 2 * R - 1)):
-        for sign in (1, -1):
-            ring_send(k, sign).start()
+    def send_decays():
+        for d in range(1, Z):
+            to = (z + d) % Z
+            remote(
+                own_row.at[:, pl.ds(pl.multiple_of(to * L, L), L)], ldb.at[z], dr_s.at[d], dr_r.at[z],
+                sp=to * X + x,
+            ).start()
+
+    own_d.wait()
+    pl.when(z > 0)(send_decays)
 
     mine = pl.ds(x * T, T)
     targets = [(x + d) % X for d in ((2, 1, 3) if X == 4 else range(1, X))]
-    for n in range(N):
-        heads, g = X * (n // G), n % G
+
+    def send_keys(n):
+        heads, g = X * (J - 1 - n // G), n % G
         for m, hbm in enumerate((k_hbm, v_hbm)):
             for to in targets:
                 remote(
                     hbm.at[g, to + heads], kv.at[n, m, mine], kv_s.at[n], kv_r.at[n], sp=z * X + to
                 ).start()
+
+    send_keys(0)
+    for k in range(min(2, 2 * R - 1)):
+        for sign in (1, -1):
+            ring_send(k, sign).start()
+    for n in range(1, N):
+        send_keys(n)
     stay = []
     for j in range(J):
-        items = pl.ds(j * G, G)
+        items = pl.ds((J - 1 - j) * G, G)
         for m, hbm in enumerate((k_hbm, v_hbm, q_hbm)):
             dst = qb.at[items, mine] if m == 2 else kv.at[items, m, mine]
             stay.append(pltpu.make_async_copy(hbm.at[:, x + X * j], dst, loc_x.at[j, m]))
             stay[-1].start()
 
-
-    for d in range(1, Z):
-        to = (z + d) % Z
-        remote(ld_hbm, ldb.at[z], dr_s.at[d], dr_r.at[z], sp=to * X + x).start()
     remote(w_hbm, wb.at[dp], p_s.at[y], p_r.at[y], dp=mate).start()
 
     for j in range(J):
         for to in targets:
             remote(
-                q_hbm.at[:, to + X * j], qb.at[pl.ds(j * G, G), mine], q_s.at[j], q_r.at[j],
+                q_hbm.at[:, to + X * (J - 1 - j)], qb.at[pl.ds(j * G, G), mine], q_s.at[j], q_r.at[j],
                 sp=z * X + to,
             ).start()
 
@@ -133,26 +149,55 @@
     cosb[...] = jnp.cos(angle)
     sinb[...] = jnp.sin(angle)
 
-    for d in range(1, Z):
-        take(ldb.at[(z + d) % Z], dr_r.at[(z + d) % Z])
-    own_d.wait()
+    ldb[z] = own_row[:, pl.ds(pl.multiple_of(z * L, L), L)]
+
+    def decays(rows):
+        run = jnp.concatenate([ldb[rows[i % len(rows)]] for i in range(8)], axis=0)
+        lane = lax.broadcasted_iota(jnp.int32, (8, L), 1)
+        step = 1
+        while step < L:
+            run = run + jnp.where(lane >= step, pltpu.roll(run, step, 1), 0.0)
+            step *= 2
+        cols = jnp.transpose(run)
+        for k, i in enumerate(rows):
+            wrow[i] = run[k : k + 1]
+            wcol[i] = jnp.broadcast_to(cols[:, k : k + 1], (L, LANES))
+
+    def rows_in(rows):
+        for i in rows:
+
+            @pl.when(z != i)
+            def _(i=i):
+                take(ldb.at[i], dr_r.at[i])
+
+    first = J - 1
+
+    @pl.when(z == 0)
+    def _():
+        rows_in(range(1, Z))
+        send_decays()
+
+    @pl.when(z > 0)
+    def _():
+        rows_in([first] if first > 0 else [])
+
+    decays([first])
+
+    def middle_decays():
+        rows = [i for i in range(1, Z) if i != first]
+        pl.when(z > 0)(lambda: rows_in(rows))
+        if rows:
+            decays(rows)
+
+    def last_decays():
+        pl.when(z > 0)(lambda: rows_in([0]))
+        decays([0])
+
     for copy in stay:
         copy.wait()
 
-    here = pl.ds(pl.multiple_of(z * L, L), L)
-    run = jnp.concatenate([ldb[i, :, here] for i in range(Z)], axis=0)
-    lane = lax.broadcasted_iota(jnp.int32, (Z, L), 1)
-    step = 1
-    while step < L:
-        run = run + jnp.where(lane >= step, pltpu.roll(run, step, 1), 0.0)
-        step *= 2
-    cols = jnp.transpose(run)
-    for i in range(Z):
-        wrow[i] = run[i : i + 1]
-        wcol[i] = jnp.broadcast_to(cols[:, i : i + 1], (L, LANES))
-
     def decay_row(n):
-        return J * (n % G) + n // G
+        return J * (n % G) + J - 1 - n // G
 
     def rotate(block):
         a, b = block[:, :LANES].astype(F32), block[:, LANES:].astype(F32)
@@ -220,7 +265,7 @@
         loc[...] = jnp.dot(weights, kv[n, 1], preferred_element_type=F32)
 
     def outputs(n):
-        s, j = n % G, n // G
+        s, j = n % G, J - 1 - n // G
         grow = jnp.exp(wcol[decay_row(n)])
         carried = jnp.dot(qb[n], s_in[n], preferred_element_type=F32)
         both = []
@@ -239,7 +284,7 @@
             ).start()
         o_rcv[j, x, rows, :] = o_snd[n, pl.ds(x * T, T), :]
 
-    lag = jnp.minimum(2 * (Z - 1 - z), N)
+    lag = jnp.where(z == Z - 1, 0, jnp.minimum(Z + 1 - z, N))
     last = N + Z
 
     def due(k):
@@ -254,6 +299,10 @@
             def _(k=k):
                 ring_step(k)
 
+        if Z > 1:
+            pl.when(t == 1)(middle_decays)
+            pl.when(t == G)(last_decays)
+
         n = jnp.clip(t - lag, 0, N - 1)
         leaving = (t >= lag) & (t < lag + N)
 
@@ -261,13 +310,17 @@
         def _():
             keys_in(jnp.minimum(t, N - 1))
 
-        @pl.when(leaving)
+        @pl.when(leaving & (z == Z - 1))
         def _():
             outputs_local(n)
 
         @pl.when(t < N)
         def _():
             chain(jnp.minimum(t, N - 1))
+
+        @pl.when(leaving & (z < Z - 1))
+        def _():
+            outputs_local(n)
 
         @pl.when(leaving)
         def _():
@@ -284,7 +337,7 @@
             total = term if total is None else total + term
         return total
 
-    for j in range(J):
+    for at, j in enumerate(reversed(range(J))):
         for d in range(1, X):
             src = (x + d) % X
             take(o_rcv.at[j, src], o_r.at[j, src])
@@ -292,12 +345,12 @@
         @pl.loop(0, Y)
         def _(k):
             yy = (y + Y + (1 - 2 * ((k + 1) % 2)) * ((k + 1) // 2)) % Y
-            if j == 0:
+            if at == 0:
                 take(wb.at[0], p_r.at[yy])
             total = project(j, yy)
-            if j > 0:
+            if at > 0:
                 total = total + acc[yy]
-            if j < J - 1:
+            if at < J - 1:
                 acc[yy] = total
             else:
                 cols2 = pl.ds(pl.multiple_of(yy * 2 * LANES, 2 * LANES), 2 * LANES)
@@ -352,7 +405,8 @@
         scratch_shapes=[
             pltpu.VMEM((N, 2, L, D), BF16),
             pltpu.VMEM((N, L, D), BF16),
-            pltpu.VMEM((Z, 1, Z * L), F32),
+            pltpu.VMEM((1, Z * L), F32),
+            pltpu.VMEM((Z, 1, L), F32),
             pltpu.VMEM((L, LANES), F32),
             pltpu.VMEM((L, LANES), F32),
             pltpu.VMEM((Z, 1, L), F32),

time: 68.2 us -> 67.9 us (level)
  the two profiles are of different devices: /device:TPU:448 before, /device:TPU:384 now
where the time goes in v3:
time: 67.9 us; the launch traced here: 67.7 us
  Pallas kernels  65.4 us (96%)
  local copies, waits for them, and re-layouts  2.3 us (3%)
    pallas_call x1, Pallas kernels, on_device(): pl.pallas_call(functools.partial(kernel, (X, Z, Y, G, J, T, D)), out_shap...  65.4 us
    unnamed x1, local copies, waits for them, and re-layouts  2.3 us

profile of v3, /device:TPU:384, one launch (start us, length us, event | category | flops | bytes accessed | tf_op | source)
XLA Modules:
  0.0 67.7 jit_solution(8545505865611496175)
XLA Ops:
  0.0 65.4 %retention.1 = bf16[256,2048]{1,0:T(8,128)(2,1)} custom-call(bf16[4,8,64,256]{3,2,1,0:T(8,128)(2,1)} %q_hbm.1, bf16[4,8,64,256]{3,2,1,0:T(8,128)(2,1)} %k_hbm.1, bf16[4,8,64,256]{3,2,1,0:T(8,128)(2,1)} %v_hbm.1, f32[1,2048]{1,0:T(1,128)} %ld_hbm.1, bf16[2048,128]{1,0:T(8,128)(2,1)} %bitcast.3, f32[1,128]{1,0:T(1,128)} %constant.7.freq_hbm), custom_call_target="tpu_custom_call" | custom-call | tf_op jit(solution)/shard_map/retention/pallas_call | solution.py:400
  65.4 2.3 %copy.8 = bf16[4,64,2048]{2,1,0:T(8,128)(2,1)} copy(bf16[4,64,2048]{2,1,0:T(8,128)(2,1)} %bitcast.2) | data formatting | bytes 2097152
